TPU v7x, 32 devices: a whole 2x2x4 slice. The times are simulated.
32 devices in a mesh: grp: 2 (over y), sp: 4 (over z), tp: 4 (over x, core).
Axes of the slice: x: 2, y: 2, z: 4, core: 2. Of those that a mesh axis runs over, the one named last changes fastest.
Arguments:
- queries: bfloat16 [2048, 2048], P(('grp', 'sp'), 'tp'), parts along dimension 0, may hold values from -6 to 6
- keys: bfloat16 [2048, 2048], P(('grp', 'sp'), 'tp'), parts along dimension 0, may hold values from -6 to 6
- values: bfloat16 [2048, 2048], P(('grp', 'sp'), 'tp'), parts along dimension 0, may hold values from -8 to 8
- offsets: float32 [16], P('tp'), as said below
- residual: bfloat16 [2048, 4096], P(('grp', 'sp', 'tp')), parts along dimension 0, may hold values from -6 to 6
- out_weight: bfloat16 [2048, 4096], P('tp'), may hold values from -0.52734375 to 0.52734375
- gain_one: float32 [4096], replicated, may hold values from 0.1 to 1.9
- shift_one: float32 [4096], replicated, may hold values from -3 to 3
- gain_two: float32 [4096], replicated, may hold values from 0.1 to 1.9
- shift_two: float32 [4096], replicated, may hold values from -3 to 3
- group_prob: float32 [2048], P(('grp', 'sp', 'tp')), parts along dimension 0, may hold values from 0.2 to 1
- pair_logits: float32 [2048, 2], P(('grp', 'sp', 'tp')), parts along dimension 0, may hold values from -6 to 6
- routes: int32 [2048, 2], P(('grp', 'sp', 'tp')), parts along dimension 0, may hold values from 0 to 15, as said below
- w_gate: bfloat16 [16, 4096, 256], P(('sp', 'tp')), may hold values from -0.09375 to 0.09375
- w_up: bfloat16 [16, 4096, 256], P(('sp', 'tp')), may hold values from -0.09375 to 0.09375
- w_down: bfloat16 [16, 256, 4096], P(('sp', 'tp')), may hold values from -1.5 to 1.5
Outputs:
- layer_out: bfloat16 [2048, 4096], P(('grp', 'sp', 'tp')), parts along dimension 0
There are 2 independent parts, one for each index of `grp`. A program takes and returns all parts, laid end to end along the dimension named above; an argument that names none is the same for every part. Nothing has to cross between parts.
Inputs may be any that keep to these rules, and one draw needn't show every extreme that they name: `routes`: both experts of a token are different and lie in one group of 4 consecutive experts. Of the tokens of one device (64 consecutive ones), at most 16 name any one expert; in every draw some experts are named exactly 16 times by the tokens of every device. `offsets`: each offset lies between 2.5 and ln(1024) - 0.3.
All inputs are finite; a program needn't handle non-finite values.
Results may differ from a plain program's by a relative error of at most 0.014.
Values may be sent and summed in bfloat16 or wider, within the bound.
A program may use at most 128 MiB of HBM per device.

v0:
```python
import math

import jax
import jax.numpy as jnp
from jax import lax
from jax.sharding import PartitionSpec as P

HEAD_DIM = 128
GROUPS = 4
TOPK = 2


residual_scale = 8.0**0.25
norm_eps = 1e-05


def layer_norm(rows, gain, shift):
    mean = jnp.mean(rows, axis=-1, keepdims=True)
    centred = rows - mean
    variance = jnp.mean(centred * centred, axis=-1, keepdims=True)
    return centred * lax.rsqrt(variance + norm_eps) * gain + shift


def slot_index(routes, expert_count, capacity):
    flat = routes.reshape(-1)
    onehot = (flat[:, None] == jnp.arange(expert_count, dtype=jnp.int32)[None, :]).astype(jnp.int32)
    earlier = jnp.cumsum(onehot, axis=0) - onehot
    rank = jnp.sum(earlier * onehot, axis=1)
    return flat * capacity + rank


def expert_rows(rows, gate_w, up_w, down_w):
    gate = jnp.dot(rows, gate_w, preferred_element_type=jnp.float32)
    upper = jnp.dot(rows, up_w, preferred_element_type=jnp.float32)
    hidden = (jax.nn.silu(gate) * upper).astype(jnp.bfloat16)
    return jnp.dot(hidden, down_w, preferred_element_type=jnp.float32).astype(jnp.bfloat16)


def per_device(
    queries,
    keys,
    values,
    offsets,
    residual,
    out_weight,
    gain_one,
    shift_one,
    gain_two,
    shift_two,
    group_prob,
    pair_logits,
    routes,
    w_gate,
    w_up,
    w_down,
):
    row_count = queries.shape[0]
    head_count = offsets.shape[0]
    block_count = lax.axis_size("sp")
    own_start = lax.axis_index("sp") * row_count
    query_pos = own_start + jnp.arange(row_count, dtype=jnp.int32)
    last_query = jnp.max(query_pos)
    query_heads = queries.reshape(row_count, head_count, HEAD_DIM)
    score_scale = HEAD_DIM ** (-0.5)

    def scores(piece, start):
        key_heads = piece.reshape(piece.shape[0], head_count, HEAD_DIM)
        score = (
            jnp.einsum("qhd,khd->hqk", query_heads, key_heads, preferred_element_type=jnp.float32)
            * score_scale
            - offsets[:, None, None]
        )
        key_pos = start + jnp.arange(piece.shape[0], dtype=jnp.int32)
        strict = key_pos[None, :] < query_pos[:, None]
        keep = jnp.where(strict, jax.nn.log_sigmoid(-score), 0.0)
        return (score, strict, keep)

    def add_totals(totals, piece, start):

        def compute(current):
            score, strict, keep = scores(piece, start)
            count = piece.shape[0] // row_count
            sums = jnp.sum(keep.reshape(head_count, row_count, count, row_count), axis=3)
            first = start // row_count
            old = lax.dynamic_slice_in_dim(current, first, count, 2)
            return lax.dynamic_update_slice_in_dim(current, old + sums, first, 2)

        return lax.cond(start < last_query, compute, lambda current: current, totals)

    def value_adder(prefix, total):

        def add_values(acc, pieces, start):
            key_piece, value_piece = pieces

            def compute(current):
                score, strict, keep = scores(key_piece, start)
                base = lax.dynamic_slice_in_dim(prefix, start // row_count, 1, 2)
                later = total[:, :, None] - base - jnp.cumsum(keep, axis=2)
                weight = jnp.where(strict, jnp.exp(jax.nn.log_sigmoid(score) + later), 0.0).astype(
                    jnp.bfloat16
                )
                value_heads = value_piece.reshape(value_piece.shape[0], head_count, HEAD_DIM)
                return current + jnp.einsum(
                    "hqk,khd->qhd", weight, value_heads, preferred_element_type=jnp.float32
                )

            return lax.cond(start < last_query, compute, lambda current: current, acc)

        return add_values

    empty_totals = jnp.zeros((head_count, row_count, block_count), jnp.float32)
    empty_out = jnp.zeros((row_count, head_count, HEAD_DIM), jnp.float32)
    every_key, every_value = (
        lax.all_gather(keys, "sp", axis=0, tiled=True),
        lax.all_gather(values, "sp", axis=0, tiled=True),
    )
    per_turn = math.gcd(block_count, max(1, 2048 // row_count))
    span_rows = per_turn * row_count

    def run_local(fold, init, operands, single):

        def step(turn, carry):
            start = (turn * span_rows).astype(jnp.int32)
            pieces = tuple(
                (lax.dynamic_slice_in_dim(operand, start, span_rows, 0) for operand in operands)
            )
            return fold(carry, pieces[0] if single else pieces, start)

        return lax.fori_loop(0, block_count // per_turn, step, init)

    totals = run_local(add_totals, empty_totals, (every_key,), True)
    prefix = jnp.cumsum(totals, axis=2) - totals
    total = jnp.sum(totals, axis=2)
    attended = run_local(value_adder(prefix, total), empty_out, (every_key, every_value), False)
    attended_rows = attended.reshape(row_count, head_count * HEAD_DIM).astype(jnp.bfloat16)
    local_rows = residual.shape[0]
    mixed = lax.psum_scatter(
        jnp.dot(attended_rows, out_weight, preferred_element_type=jnp.float32).astype(jnp.bfloat16),
        "tp",
        scatter_dimension=0,
        tiled=True,
    ).astype(jnp.float32)
    normed = layer_norm(
        residual_scale * residual.astype(jnp.float32) + mixed, gain_one, shift_one
    ).astype(jnp.bfloat16)
    width = normed.shape[1]
    expert_count = lax.axis_size("sp") * lax.axis_size("tp")
    capacity = local_rows // (expert_count // GROUPS)
    slots = slot_index(routes, expert_count, capacity)
    buffer = (
        jnp.zeros((expert_count * capacity, width), jnp.bfloat16)
        .at[slots]
        .set(jnp.repeat(normed, TOPK, axis=0))
    )
    arrived = lax.all_to_all(
        buffer.reshape(expert_count, capacity, width),
        ("sp", "tp"),
        split_axis=0,
        concat_axis=0,
        tiled=True,
    )
    result = expert_rows(arrived.reshape(-1, width), w_gate[0], w_up[0], w_down[0]).reshape(
        expert_count, capacity, width
    )
    returned = lax.all_to_all(result, ("sp", "tp"), split_axis=0, concat_axis=0, tiled=True)
    picked = returned.reshape(-1, width)[slots].reshape(local_rows, TOPK, width)
    difference = pair_logits[:, 0] - pair_logits[:, 1]
    pair_weight = jnp.stack([jax.nn.sigmoid(difference), jax.nn.sigmoid(-difference)], axis=1)
    route_weight = group_prob[:, None] * pair_weight
    moe = jnp.sum(route_weight[:, :, None] * picked.astype(jnp.float32), axis=1)
    return layer_norm(
        residual_scale * normed.astype(jnp.float32) + moe, gain_two, shift_two
    ).astype(jnp.bfloat16)


def solution(mesh):
    return jax.shard_map(
        per_device,
        mesh=mesh,
        in_specs=(
            P(("grp", "sp"), "tp"),
            P(("grp", "sp"), "tp"),
            P(("grp", "sp"), "tp"),
            P("tp"),
            P(("grp", "sp", "tp"), None),
            P("tp", None),
            P(),
            P(),
            P(),
            P(),
            P(("grp", "sp", "tp")),
            P(("grp", "sp", "tp"), None),
            P(("grp", "sp", "tp"), None),
            P(("sp", "tp"), None, None),
            P(("sp", "tp"), None, None),
            P(("sp", "tp"), None, None),
        ),
        out_specs=P(("grp", "sp", "tp"), None),
        check_vma=False,
    )
```

profile of v0, /device:TPU:11, one launch (start us, length us, event | category | flops | bytes accessed | tf_op | source)
XLA Modules:
  0.0 292.9 jit_solution(13146834701542293893)
XLA Ops:
  6.5 0.7 all-gather.3.cloned.1.call-update
  7.3 0.7 all-gather.5.cloned.1.call-update
  8.1 1.1 copy.46
  9.2 0.6 fusion.53
  10.4 26.8 %all-gather.3.cloned.1.call-done = bf16[1024,512]{1,0:T(8,128)(2,1)} async-done(((bf16[256,512]{1,0:T(8,128)(2,1)}), bf16[1024,512]{1,0:T(8,128)(2,1)}) %all-gather.3.cloned.1.call-update) | async-done | bytes 1048592 | tf_op jit(solution)/shard_map/all_gather | solution.py:114
  37.3 15.8 %conditional.2 = (f32[4,256,4]{2,1,0:T(8,128)S(1)}) conditional(s32[]{:T(128)} %convert_element_type.55, f32[4,256,4]{2,1,0:T(8,128)S(1)} %broadcast_in_dim.32, (s32[256]{0:T(256)S(1)}, bf16[1024,512]{1,0:T(8,128)(2,1)}, bf16[256,4,128]{0,2,1:T(8,128)(2,1)S(1)}, f32[4]{0:T(128)}, f32[4,256,4]{2,1,0:T(8,128)S(1)}) %tuple.62), branch_computations={%region_1.2_spmd, %region_2.4_spmd} | conditional | flops 280231936 | bytes 18678812 | solution.py:88
  37.3 0.2 iota_compare_fusion
  37.5 6.5 %fusion.1 = f32[4,256,1024]{2,1,0:T(8,128)} fusion(bf16[256,4,128]{0,2,1:T(8,128)(2,1)S(1)} %get-tuple-element.158, f32[4]{0:T(128)} %get-tuple-element.119, pred[256,1024]{1,0:T(8,128)(4,1)S(1)} %iota_compare_fusion, bf16[1024,512]{1,0:T(8,128)(2,1)} %get-tuple-element.118), kind=kOutput, calls=%fused_computation.4 | convolution fusion | flops 278921216 | bytes 5767184 | tf_op jit(solution)/shard_map/while/body/eval_jaxpr/cond/branch_1_fun/qhd,khd->hqk/dot_general | solution.py:69
  44.0 5.6 %reshape.140 = f32[4,256,4,256]{3,2,1,0:T(4,128)} reshape(f32[4,256,1024]{2,1,0:T(8,128)} %fusion.1) | data formatting | bytes 8388608 | tf_op jit(solution)/shard_map/while/body/eval_jaxpr/cond/branch_1_fun/reshape | solution.py:83
  49.6 3.4 %reduce_sum.71 = f32[4,256,4]{2,1,0:T(8,128)S(1)} reduce(f32[4,256,4,256]{3,2,1,0:T(4,128)} %reshape.140, f32[]{:T(128)} %constant.81.clone), dimensions={3}, to_apply=%region_3.3 | reduce | flops 1044480 | bytes 4210692 | tf_op jit(solution)/shard_map/while/body/eval_jaxpr/cond/branch_1_fun/reduce_sum | solution.py:83
  53.1 0.2 copy.48
  53.3 12.9 %all-gather.5.cloned.1.call-done = bf16[1024,512]{1,0:T(8,128)(2,1)} async-done(((bf16[256,512]{1,0:T(8,128)(2,1)}), bf16[1024,512]{1,0:T(8,128)(2,1)}) %all-gather.5.cloned.1.call-update) | async-done | bytes 1048592 | tf_op jit(solution)/shard_map/all_gather | solution.py:115
  66.2 42.3 %conditional.3 = (f32[256,4,128]{2,0,1:T(8,128)S(1)}) conditional(s32[]{:T(128)} %convert_element_type.55, f32[256,4,128]{2,0,1:T(8,128)S(1)} %broadcast_in_dim.31, (s32[256]{0:T(256)S(1)}, bf16[1024,512]{1,0:T(8,128)(2,1)}, bf16[256,4,128]{0,2,1:T(8,128)(2,1)S(1)}, f32[4]{0:T(128)}, f32[4,256,4]{2,1,0:T(8,128)S(1)}, ...), branch_computations={%region_6.7_spmd, %region_7.10_spmd} | conditional | flops 696717312 | bytes 90485984 | solution.py:107
  66.4 0.2 iota_compare_fusion.1
  66.6 6.5 %fusion.10 = (f32[4,256,1024]{2,1,0:T(8,128)S(1)}, f32[4,256,1024]{2,1,0:T(8,128)}) fusion(f32[4]{0:T(128)} %get-tuple-element.124, pred[256,1024]{1,0:T(8,128)(4,1)S(1)} %iota_compare_fusion.1, bf16[256,4,128]{0,2,1:T(8,128)(2,1)S(1)} %get-tuple-element.163, bf16[1024,512]{1,0:T(8,128)(2,1)} %get-tuple-element.123), kind=kOutput, calls=%fused_computation.16 | convolution fusion | flops 278921216 | bytes 9961488 | tf_op jit(solution)/shard_map/while/body/eval_jaxpr/cond/branch_1_fun/qhd,khd->hqk/dot_general | solution.py:69
  73.1 3.0 %copy.62 = f32[128,8,8,128]{3,2,1,0:T(8,128)} copy(f32[128,8,8,128]{3,1,2,0:T(8,128)S(1)} %bitcast.79) | data formatting | bytes 8388608 | tf_op jit(solution)/shard_map/while/body/eval_jaxpr/cond
  76.1 5.5 %copy.43 = f32[4,256,8,128]{1,2,3,0:T(8,128)} copy(f32[4,256,8,128]{3,2,1,0:T(8,128)} %bitcast.76) | data formatting | bytes 8388608 | tf_op jit(solution)/shard_map/reshape
  81.6 2.5 fusion.55
  84.2 2.0 copy-done.2
  86.2 4.5 %broadcast_add_fusion = f32[4,256,8,128]{1,2,3,0:T(8,128)} fusion(f32[4,256,8,128]{1,2,3,0:T(8,128)} %copy-done.2, f32[4,256,8]{1,2,0:T(8,128)S(1)} %slice.20), kind=kLoop, calls=%fused_computation.18 | loop fusion | flops 1048576 | bytes 8421376 | tf_op jit(solution)/shard_map/reduce_window_sum
  90.7 5.5 %copy.44 = f32[4,256,8,128]{3,2,1,0:T(8,128)} copy(f32[4,256,8,128]{1,2,3,0:T(8,128)} %broadcast_add_fusion) | data formatting | bytes 8388608 | tf_op jit(solution)/shard_map/reduce_window_sum
  96.2 5.0 %reduce_window_sum.34 = f32[4,256,1024]{2,1,0:T(8,128)} reshape(f32[4,256,8,128]{3,2,1,0:T(8,128)} %copy.44) | data formatting | bytes 8388608 | tf_op jit(solution)/shard_map/reduce_window_sum
  101.2 0.2 copy.51
  101.3 0.2 reduce_sum.88
  101.6 6.7 %fusion.16 = f32[256,4,128]{2,0,1:T(8,128)S(1)} fusion(f32[256,4,128]{2,0,1:T(8,128)S(1)} %get-tuple-element.120, f32[4,256,1024]{2,1,0:T(8,128)} %reduce_window_sum.34, f32[4,256,1024]{2,1,0:T(8,128)} %get-tuple-element.172, f32[4,256]{1,0:T(4,128)S(1)} %fusion.25, f32[4]{0:T(128)S(1)} %copy-done.14, pred[256,1024]{1,0:T(8,128)(4,1)S(1)} %copy-done.6, ...), kind=kOutput, calls=%fused_computation.21 | convolution fusion | flops 283246592 | bytes 10752016 | tf_op jit(solution)/shard_map/while/body/eval_jaxpr/cond/branch_1_fun/hqk,khd->qhd/dot_general | solution.py:103
  108.7 4.9 %convolution_convert_fusion.1 = bf16[256,4096]{1,0:T(8,128)(2,1)} fusion(bf16[256,512]{0,1:T(8,128)(2,1)S(1)} %bitcast.80, bf16[512,4096]{1,0:T(8,128)(2,1)} %param.25), kind=kOutput, calls=%fused_computation.35 | convolution fusion | flops 1074790400 | bytes 6553600 | tf_op jit(solution)/shard_map/dot_general | solution.py:138
  113.7 0.1 eq.15
  113.9 0.2 reduce_window_sum.38
  114.3 0.2 select_reduce_fusion
  114.5 29.5 %reduce-scatter.2.cloned.1.call-done = bf16[64,4096]{1,0:T(8,128)(2,1)} async-done(((bf16[256,4096]{1,0:T(8,128)(2,1)}), bf16[64,4096]{1,0:T(8,128)(2,1)}) %reduce-scatter.2.cloned.1.call-update) | async-done | bytes 524304 | tf_op jit(solution)/shard_map/reduce_scatter | solution.py:137
  144.1 1.3 fusion.43
  145.4 1.4 multiply_reduce_fusion.2
  146.8 1.3 add_convert_fusion.1
  148.2 2.0 broadcast_in_dim.34
  150.2 2.3 reshape.170
  152.4 4.3 %scatter_custom_fusion = bf16[256,4096]{1,0:T(8,128)(2,1)} fusion(s32[128]{0:T(128)S(1)} %fusion.52, bf16[128,4096]{1,0:T(8,128)(2,1)} %reshape.170, bf16[]{:T(256)} %constant.101.clone.1), kind=kCustom, calls=%fused_computation.46 | custom fusion | bytes 2097664 | tf_op jit(solution)/shard_map/scatter | solution.py:153
  156.8 53.9 %all_to_all.10 = bf16[16,16,4096]{2,1,0:T(8,128)(2,1)S(1)} all-to-all(bf16[16,16,4096]{2,1,0:T(8,128)(2,1)} %bitcast.77), channel_id=1, replica_groups=mesh['grp'=2,'sp'=4,'tp'=4] {'sp','tp'}, dimensions={0} | all-to-all | bytes 4194304 | tf_op jit(solution)/shard_map/all_to_all | solution.py:155
  210.7 1.3 copy-done.1
  212.1 0.7 fusion.31
  212.8 5.9 %convolution_convert_fusion = bf16[256,4096]{1,0:T(8,128)(2,1)} fusion(bf16[1,256,4096]{2,1,0:T(8,128)(2,1)S(1)} %copy-done, bf16[256,4096]{1,0:T(8,128)(2,1)} %bitcast.75, bf16[1,4096,256]{2,1,0:T(8,128)(2,1)} %param.34, f32[256,256]{1,0:T(8,128)S(1)} %fusion.31), kind=kOutput, calls=%fused_computation.34 | convolution fusion | flops 1075183616 | bytes 8650752 | tf_op jit(solution)/shard_map/dot_general | solution.py:36
  218.7 5.2 %all-to-all-start.1 = ((bf16[16,16,4096]{2,1,0:T(8,128)(2,1)}), bf16[16,16,4096]{2,1,0:T(8,128)(2,1)}, u32[]{:S(2)}, u32[]{:S(2)}) async-start(bf16[16,16,4096]{2,1,0:T(8,128)(2,1)} %bitcast.78), calls=%async_computation.2 | async-start | bytes 4194304 | tf_op jit(solution)/shard_map/all_to_all | solution.py:165
  224.0 47.4 %all-to-all-done.1 = bf16[16,16,4096]{2,1,0:T(8,128)(2,1)} async-done(((bf16[16,16,4096]{2,1,0:T(8,128)(2,1)}), bf16[16,16,4096]{2,1,0:T(8,128)(2,1)}, u32[]{:S(2)}, u32[]{:S(2)}) %all-to-all-start.1) | async-done | bytes 2097184 | tf_op jit(solution)/shard_map/all_to_all | solution.py:165
  271.4 5.0 %gather_fusion = bf16[128,4096]{1,0:T(8,128)(2,1)} fusion(bf16[256,4096]{1,0:T(8,128)(2,1)} %bitcast.14, s32[1024]{0:T(1024)S(1)} %pad_clamp_fusion), kind=kCustom, calls=%fused_computation | custom fusion | bytes 2097664 | tf_op jit(solution)/shard_map/gather | solution.py:166
  276.4 3.4 %reshape.157 = f32[64,2,4096]{2,1,0:T(2,128)} reshape(bf16[128,4096]{1,0:T(8,128)(2,1)} %gather_fusion) | data formatting | bytes 3145728 | tf_op jit(solution)/shard_map/convert_element_type | solution.py:170
  279.8 4.8 %multiply_reduce_fusion = f32[64,4096]{1,0:T(8,128)S(1)} fusion(f32[64,2,4096]{2,1,0:T(2,128)} %reshape.157, f32[64,2]{1,0:T(8,128)S(1)} %copy.53), kind=kLoop, calls=%fused_computation.41 | loop fusion | flops 786432 | bytes 3146240 | tf_op jit(solution)/shard_map/reduce_sum | solution.py:170
  284.6 0.3 fusion.44
  284.9 0.3 multiply_reduce_fusion.1
  285.3 1.1 add_convert_fusion
  (56 shorter events, 1.1 us)
Async XLA Ops:
  6.5 206.2 %copy-start = (bf16[1,256,4096]{2,1,0:T(8,128)(2,1)S(1)}, bf16[1,256,4096]{2,1,0:T(8,128)(2,1)}, u32[]{:S(2)}) copy-start(bf16[1,256,4096]{2,1,0:T(8,128)(2,1)} %param.35) | copy-start | bytes 6291460
  6.5 30.7 %all-gather.3.cloned.1.call-start = ((), (), s32[]{:S(2)}) async-start(), calls=%async_computation.3 | async-start | bytes 1310720 | tf_op jit(solution)/shard_map/all_gather | solution.py:114
  7.3 58.9 %all-gather.5.cloned.1.call-start = ((), (), s32[]{:S(2)}) async-start(), calls=%async_computation.4 | async-start | bytes 1310720 | tf_op jit(solution)/shard_map/all_gather | solution.py:115
  8.0 136.1 %reduce-scatter.2.cloned.1.call-start = ((), (), s32[]{:S(2)}) async-start(), calls=%async_computation.5 | async-start | bytes 2621440 | tf_op jit(solution)/shard_map/reduce_scatter | solution.py:137
  66.6 6.5 %copy-start.5 = (pred[256,1024]{1,0:T(8,128)(4,1)}, pred[256,1024]{1,0:T(8,128)(4,1)S(1)}, u32[]{:S(2)}) copy-start(pred[256,1024]{1,0:T(8,128)(4,1)S(1)} %iota_compare_fusion.1) | copy-start | bytes 786436 | tf_op jit(solution)/shard_map/while/body/eval_jaxpr/cond
  84.2 2.0 copy-start.2
  96.2 5.4 %copy-start.6 = (pred[256,1024]{1,0:T(8,128)(4,1)S(1)}, pred[256,1024]{1,0:T(8,128)(4,1)}, u32[]{:S(2)}) copy-start(pred[256,1024]{1,0:T(8,128)(4,1)} %copy-done.5) | copy-start | bytes 786436 | tf_op jit(solution)/shard_map/while/body/eval_jaxpr/cond
  96.2 5.4 %copy-start.14 = (f32[4]{0:T(128)S(1)}, f32[4]{0:T(128)}, u32[]{:S(2)}) copy-start(f32[4]{0:T(128)} %get-tuple-element.124) | copy-start | bytes 52 | tf_op jit(solution)/shard_map/while/body/eval_jaxpr/cond
  108.6 4.9 %copy-start.11 = (s32[64,2]{0,1:T(2,128)S(1)}, s32[64,2]{0,1:T(2,128)}, u32[]{:S(2)}) copy-start(s32[64,2]{0,1:T(2,128)} %param.32) | copy-start | bytes 1540
  108.6 35.4 %copy-start.3 = (bf16[64,4096]{1,0:T(8,128)(2,1)S(1)}, bf16[64,4096]{1,0:T(8,128)(2,1)}, u32[]{:S(2)}) copy-start(bf16[64,4096]{1,0:T(8,128)(2,1)} %param.24) | copy-start | bytes 1572868
  108.6 38.1 %copy-start.7 = (f32[4096]{0:T(1024)S(1)}, f32[4096]{0:T(1024)}, u32[]{:S(2)}) copy-start(f32[4096]{0:T(1024)} %param.27) | copy-start | bytes 49156
  108.7 38.1 %copy-start.8 = (f32[4096]{0:T(1024)S(1)}, f32[4096]{0:T(1024)}, u32[]{:S(2)}) copy-start(f32[4096]{0:T(1024)} %param.26) | copy-start | bytes 49156
  156.8 55.3 %copy-start.4 = (bf16[1,4096,256]{2,1,0:T(8,128)(2,1)S(1)}, bf16[1,4096,256]{2,1,0:T(8,128)(2,1)}, u32[]{:S(2)}) copy-start(bf16[1,4096,256]{2,1,0:T(8,128)(2,1)} %param.33) | copy-start | bytes 6291460
  210.7 1.4 copy-start.1
  218.7 5.2 %copy-start.12 = (f32[64,2]{0,1:T(2,128)S(1)}, f32[64,2]{0,1:T(2,128)}, u32[]{:S(2)}) copy-start(f32[64,2]{0,1:T(2,128)} %param.31) | copy-start | bytes 1540
  218.7 5.2 %copy-start.13 = (f32[64]{0:T(128)S(1)}, f32[64]{0:T(128)}, u32[]{:S(2)}) copy-start(f32[64]{0:T(128)} %param.30) | copy-start | bytes 772
  218.7 52.7 %all-to-all-start.1 = ((bf16[16,16,4096]{2,1,0:T(8,128)(2,1)}), bf16[16,16,4096]{2,1,0:T(8,128)(2,1)}, u32[]{:S(2)}, u32[]{:S(2)}) async-start(bf16[16,16,4096]{2,1,0:T(8,128)(2,1)} %bitcast.78), calls=%async_computation.2 | async-start | bytes 4194304 | tf_op jit(solution)/shard_map/all_to_all | solution.py:165
  276.4 8.8 %copy-start.9 = (f32[4096]{0:T(1024)S(1)}, f32[4096]{0:T(1024)}, u32[]{:S(2)}) copy-start(f32[4096]{0:T(1024)} %param.29) | copy-start | bytes 49156
  276.4 8.8 %copy-start.10 = (f32[4096]{0:T(1024)S(1)}, f32[4096]{0:T(1024)}, u32[]{:S(2)}) copy-start(f32[4096]{0:T(1024)} %param.28) | copy-start | bytes 49156
Sparse Core Ops, SparseCore 0:
  8.9 28.2 all-gather.2
  38.8 27.3 all-gather.4
  113.7 30.3 reduce-scatter.1
where the time goes:
time: 294 us; the launch traced here: 293 us
  waiting for transfers between devices  118 us (40%)
  blocking collectives  53.9 us (18%)
  local copies, waits for them, and re-layouts  47.3 us (16%)
  matrix products  31.1 us (11%)
  other arithmetic  22.8 us (8%)
  between operations  14 us (5%)
  starting transfers between devices  5.24 us (2%)
    all_to_all x1, blocking collectives, per_device(): lax.all_to_all(buffer.reshape(expert_count, capacity, width), ('sp', 'tp'...  53.9 us
    all_to_all x1, waiting for transfers between devices, per_device(): lax.all_to_all(result, ('sp', 'tp'), split_axis=0, concat_axis=0, tiled=T...  47.4 us
    reduce_scatter x1, waiting for transfers between devices, per_device(): lax.psum_scatter(jnp.dot(attended_rows, out_weight, preferred_element_typ...  29.5 us
    all_gather x1, waiting for transfers between devices, per_device(): lax.all_gather(keys, 'sp', axis=0, tiled=True)  26.8 us
    dot_general x2, matrix products, scores(): jnp.einsum('qhd,khd->hqk', query_heads, key_heads, preferred_element_type...  12.9 us
    all_gather x1, waiting for transfers between devices, per_device(): lax.all_gather(values, 'sp', axis=0, tiled=True)  12.9 us
    another operation x5, local copies, waits for them, and re-layouts  10.7 us
    another operation x3, other arithmetic  7.05 us
  transfers between devices with their start and end apart: 4, of which 4 were waited for; matrix products, arithmetic and copies ran while one was open for 6% of the time, Pallas kernels for 0%

commit v1 on v0

v1 whole, which is shorter than its diff:
```python
import functools

import jax
import jax.numpy as jnp
from jax import lax
from jax.experimental import pallas as pl
from jax.experimental.pallas import tpu as pltpu
from jax.sharding import PartitionSpec as P

HEAD_DIM = 128
GROUPS = 4
TOPK = 2
MESH = pl.DeviceIdType.MESH

residual_scale = 8.0**0.25
norm_eps = 1e-05


def remote(src, dst, send_sem, recv_sem, target):
    return pltpu.make_async_remote_copy(
        src_ref=src,
        dst_ref=dst,
        send_sem=send_sem,
        recv_sem=recv_sem,
        device_id=target,
        device_id_type=MESH,
    )


def norm_rows(rows, gain, shift):
    mean = jnp.mean(rows, axis=-1, keepdims=True)
    centred = rows - mean
    variance = jnp.mean(centred * centred, axis=-1, keepdims=True)
    return centred * lax.rsqrt(variance + norm_eps) * gain + shift


def attend_kernel(
    n_sp,
    n_tp,
    chunks,
    off_ref,
    q_ref,
    k_ref,
    v_ref,
    gain_ref,
    shift_ref,
    res_hbm,
    w_hbm,
    out_ref,
    kv,
    w_ref,
    res_ref,
    later_ref,
    carry,
    acc,
    att,
    send1,
    keep1,
    recv1,
    send2,
    recv2,
    rows_ref,
    load_sem,
    kv_send,
    kv_recv,
    s1,
    r1,
    s2,
    r2,
):
    me = lax.axis_index("sp")
    t = lax.axis_index("tp")
    rows = q_ref.shape[0]
    heads = q_ref.shape[1] // HEAD_DIM
    local = res_ref.shape[0]
    cols = w_ref.shape[1] // chunks
    near = t + 1 - 2 * lax.rem(t, 2)
    far = lax.rem(t + 2, 4)

    load_w = pltpu.make_async_copy(w_hbm, w_ref, load_sem.at[0])
    load_res = pltpu.make_async_copy(res_hbm, res_ref, load_sem.at[1])
    load_w.start()
    load_res.start()

    barrier = pltpu.get_barrier_semaphore()
    for step in (1, n_sp - 1):
        pl.semaphore_signal(
            barrier, inc=1, device_id={"sp": lax.rem(me + step, n_sp)}, device_id_type=MESH
        )
    for partner in (near, far):
        pl.semaphore_signal(barrier, inc=1, device_id={"tp": partner}, device_id_type=MESH)
    pl.semaphore_wait(barrier, 4)

    up = {"sp": lax.rem(me + 1, n_sp)}
    own = [
        remote(ref, kv.at[me, i], kv_send.at[me, i], kv_recv.at[me, i], up)
        for i, ref in enumerate((k_ref, v_ref))
    ]

    def passed(j, i):
        return remote(kv.at[j, i], kv.at[j, i], kv_send.at[j, i], kv_recv.at[j, i], up)

    @pl.when(me < n_sp - 1)
    def _():
        own[0].start()
        own[1].start()

    row_id = lax.broadcasted_iota(jnp.int32, (rows, rows), 0)
    col_id = lax.broadcasted_iota(jnp.int32, (rows, rows), 1)
    later_ref[...] = jnp.where(row_id > col_id, 1.0, 0.0).astype(jnp.bfloat16)
    scale = HEAD_DIM ** (-0.5)

    def block(key_of, value_of, first):
        for h in range(heads):
            span = slice(h * HEAD_DIM, (h + 1) * HEAD_DIM)
            score = (
                lax.dot_general(
                    q_ref[:, span],
                    key_of(span),
                    (((1,), (1,)), ((), ())),
                    preferred_element_type=jnp.float32,
                )
                * scale
                - off_ref[h]
            )
            soft = jnp.maximum(score, 0.0) + jnp.log(1.0 + jnp.exp(-jnp.abs(score)))
            gain = score - soft
            if first:
                soft = jnp.where(col_id < row_id, soft, 0.0)
            high = soft.astype(jnp.bfloat16)
            low = (soft - high.astype(jnp.float32)).astype(jnp.bfloat16)
            tail = jnp.dot(high, later_ref[...], preferred_element_type=jnp.float32)
            tail = tail + jnp.dot(low, later_ref[...], preferred_element_type=jnp.float32)
            total = jnp.sum(soft, axis=1, keepdims=True)
            if first:
                weight = jnp.where(col_id < row_id, jnp.exp(gain - tail), 0.0)
                carry[h] = total
            else:
                weight = jnp.exp(gain - tail - carry[h])
                carry[h] = carry[h] + total
            part = jnp.dot(
                weight.astype(jnp.bfloat16), value_of(span), preferred_element_type=jnp.float32
            )
            if first:
                acc[:, span] = part
            else:
                acc[:, span] = acc[:, span] + part

    block(lambda span: k_ref[:, span], lambda span: v_ref[:, span], True)

    def turn(step, _):
        j = me - step
        for i in range(2):
            passed(j, i).wait_recv()

            @pl.when(me < n_sp - 1)
            def _():
                passed(j, i).start()

        block(lambda span: kv[j, 0, :, span], lambda span: kv[j, 1, :, span], False)
        return 0

    lax.fori_loop(1, me + 1, turn, 0)

    att[...] = acc[...].astype(jnp.bfloat16)
    order = (
        near + 2 - 4 * (near // 2),
        near,
        far,
        t,
    )
    picked = jnp.concatenate(
        [att[pl.ds(pl.multiple_of(b * local, local), local), :] for b in order], axis=0
    )
    half = rows // 2
    load_w.wait()
    load_res.wait()

    def hop1(c):
        return remote(send1.at[c], recv1.at[c], s1.at[c], r1.at[c], {"tp": near})

    def hop2(c):
        return remote(send2.at[c], recv2.at[c], s2.at[c], r2.at[c], {"tp": far})

    for c in range(chunks):
        part = jnp.dot(
            picked, w_ref[:, c * cols : (c + 1) * cols], preferred_element_type=jnp.float32
        ).astype(jnp.bfloat16)
        send1[c] = part[:half]
        keep1[c] = part[half:]
        hop1(c).start()
    for c in range(chunks):
        hop1(c).wait_recv()
        both = keep1[c].astype(jnp.float32) + recv1[c].astype(jnp.float32)
        send2[c] = both[:local].astype(jnp.bfloat16)
        hop2(c).start()
        span = slice(c * cols, (c + 1) * cols)
        rows_ref[:, span] = (
            residual_scale * res_ref[:, span].astype(jnp.float32) + both[local:]
        )
    for c in range(chunks):
        hop2(c).wait_recv()
        span = slice(c * cols, (c + 1) * cols)
        rows_ref[:, span] = rows_ref[:, span] + recv2[c].astype(jnp.float32)
    out_ref[...] = norm_rows(rows_ref[...], gain_ref[...], shift_ref[...]).astype(jnp.bfloat16)

    for c in range(chunks):
        hop1(c).wait_send()
        hop2(c).wait_send()

    @pl.when(me < n_sp - 1)
    def _():
        own[0].wait_send()
        own[1].wait_send()

        def drain(step, _):
            for i in range(2):
                passed(me - step, i).wait_send()
            return 0

        lax.fori_loop(1, me + 1, drain, 0)


def attend(queries, keys, values, offsets, residual, out_weight, gain, shift):
    n_sp, n_tp = lax.axis_size("sp"), lax.axis_size("tp")
    assert n_tp == 4
    rows, inner = queries.shape
    local, width = residual.shape
    heads = offsets.shape[0]
    chunks = 8
    cols = width // chunks
    half = rows // 2
    vmem = pl.BlockSpec(memory_space=pltpu.VMEM)
    hbm = pl.BlockSpec(memory_space=pl.ANY)
    dma = pltpu.SemaphoreType.DMA
    bf16, f32 = jnp.bfloat16, jnp.float32
    return pl.pallas_call(
        functools.partial(attend_kernel, n_sp, n_tp, chunks),
        out_shape=jax.ShapeDtypeStruct((local, width), bf16),
        in_specs=[pl.BlockSpec(memory_space=pltpu.SMEM), vmem, vmem, vmem, vmem, vmem, hbm, hbm],
        out_specs=vmem,
        scratch_shapes=[
            pltpu.VMEM((n_sp, 2, rows, inner), bf16),
            pltpu.VMEM(out_weight.shape, bf16),
            pltpu.VMEM(residual.shape, bf16),
            pltpu.VMEM((rows, rows), bf16),
            pltpu.VMEM((heads, rows, 1), f32),
            pltpu.VMEM((rows, inner), f32),
            pltpu.VMEM((rows, inner), bf16),
            pltpu.VMEM((chunks, half, cols), bf16),
            pltpu.VMEM((chunks, half, cols), bf16),
            pltpu.VMEM((chunks, half, cols), bf16),
            pltpu.VMEM((chunks, local, cols), bf16),
            pltpu.VMEM((chunks, local, cols), bf16),
            pltpu.VMEM((local, width), f32),
            dma((2,)),
            dma((n_sp, 2)),
            dma((n_sp, 2)),
            dma((chunks,)),
            dma((chunks,)),
            dma((chunks,)),
            dma((chunks,)),
        ],
        compiler_params=pltpu.CompilerParams(collective_id=0, has_side_effects=True),
        name="attend",
    )(offsets, queries, keys, values, gain[None], shift[None], residual, out_weight)


def layer_norm(rows, gain, shift):
    mean = jnp.mean(rows, axis=-1, keepdims=True)
    centred = rows - mean
    variance = jnp.mean(centred * centred, axis=-1, keepdims=True)
    return centred * lax.rsqrt(variance + norm_eps) * gain + shift


def slot_index(routes, expert_count, capacity):
    flat = routes.reshape(-1)
    onehot = (flat[:, None] == jnp.arange(expert_count, dtype=jnp.int32)[None, :]).astype(jnp.int32)
    earlier = jnp.cumsum(onehot, axis=0) - onehot
    rank = jnp.sum(earlier * onehot, axis=1)
    return flat * capacity + rank


def expert_rows(rows, gate_w, up_w, down_w):
    gate = jnp.dot(rows, gate_w, preferred_element_type=jnp.float32)
    upper = jnp.dot(rows, up_w, preferred_element_type=jnp.float32)
    hidden = (jax.nn.silu(gate) * upper).astype(jnp.bfloat16)
    return jnp.dot(hidden, down_w, preferred_element_type=jnp.float32).astype(jnp.bfloat16)


def per_device(
    queries,
    keys,
    values,
    offsets,
    residual,
    out_weight,
    gain_one,
    shift_one,
    gain_two,
    shift_two,
    group_prob,
    pair_logits,
    routes,
    w_gate,
    w_up,
    w_down,
):
    normed = attend(
        queries, keys, values, offsets, residual, out_weight, gain_one, shift_one
    )
    local_rows = residual.shape[0]
    width = normed.shape[1]
    expert_count = lax.axis_size("sp") * lax.axis_size("tp")
    capacity = local_rows // (expert_count // GROUPS)
    slots = slot_index(routes, expert_count, capacity)
    buffer = (
        jnp.zeros((expert_count * capacity, width), jnp.bfloat16)
        .at[slots]
        .set(jnp.repeat(normed, TOPK, axis=0))
    )
    arrived = lax.all_to_all(
        buffer.reshape(expert_count, capacity, width),
        ("sp", "tp"),
        split_axis=0,
        concat_axis=0,
        tiled=True,
    )
    result = expert_rows(arrived.reshape(-1, width), w_gate[0], w_up[0], w_down[0]).reshape(
        expert_count, capacity, width
    )
    returned = lax.all_to_all(result, ("sp", "tp"), split_axis=0, concat_axis=0, tiled=True)
    picked = returned.reshape(-1, width)[slots].reshape(local_rows, TOPK, width)
    difference = pair_logits[:, 0] - pair_logits[:, 1]
    pair_weight = jnp.stack([jax.nn.sigmoid(difference), jax.nn.sigmoid(-difference)], axis=1)
    route_weight = group_prob[:, None] * pair_weight
    moe = jnp.sum(route_weight[:, :, None] * picked.astype(jnp.float32), axis=1)
    return layer_norm(
        residual_scale * normed.astype(jnp.float32) + moe, gain_two, shift_two
    ).astype(jnp.bfloat16)


def solution(mesh):
    return jax.shard_map(
        per_device,
        mesh=mesh,
        in_specs=(
            P(("grp", "sp"), "tp"),
            P(("grp", "sp"), "tp"),
            P(("grp", "sp"), "tp"),
            P("tp"),
            P(("grp", "sp", "tp"), None),
            P("tp", None),
            P(),
            P(),
            P(),
            P(),
            P(("grp", "sp", "tp")),
            P(("grp", "sp", "tp"), None),
            P(("grp", "sp", "tp"), None),
            P(("sp", "tp"), None, None),
            P(("sp", "tp"), None, None),
            P(("sp", "tp"), None, None),
        ),
        out_specs=P(("grp", "sp", "tp"), None),
        check_vma=False,
    )
```

time: 294 us -> 194 us (0.66)
  waiting for transfers between devices: 118 us -> 47.4 us
  Pallas kernels: 0 us -> 33.9 us
  local copies, waits for them, and re-layouts: 47.3 us -> 16.9 us
  matrix products: 31.1 us -> 6.65 us
  blocking collectives: 53.9 us -> 75.4 us
  other arithmetic: 22.8 us -> 7.64 us
  between operations: 14 us -> 0.14 us
    all_gather x2 -> x0, waiting for transfers between devices: 39.6 us -> none  [the longest x1 26.8 us: per_device(): lax.all_gather(keys, 'sp', axis=0, tiled=True)]
    pallas_call x0 -> x1, Pallas kernels: none -> 33.9 us  [attend(): pl.pallas_call(functools.partial(attend_kernel, n_sp, n_tp, chunks), out_...]
    reduce_scatter x1 -> x0, waiting for transfers between devices: 29.5 us -> none  [per_device(): lax.psum_scatter(jnp.dot(attended_rows, out_weight, preferred_element_typ...]
    dot_general x4 -> x0, matrix products: 24.5 us -> none  [the longest x2 12.9 us: scores(): jnp.einsum('qhd,khd->hqk', query_heads, key_heads, preferred_element_type...]
    all_to_all x1, blocking collectives: 53.9 us -> 75.4 us  [per_device(): lax.all_to_all(buffer.reshape(expert_count, capacity, width), ('sp', 'tp'...]
    reshape x2 -> x0, local copies, waits for them, and re-layouts: 11.2 us -> none  [the longest x1 5.63 us: compute(): keep.reshape(head_count, row_count, count, row_count)]
    another operation x5 -> x0, local copies, waits for them, and re-layouts: 10.7 us -> none
    another operation x4 -> x0, other arithmetic: 7.06 us -> none
  transfers between devices with their start and end apart: 4 -> 1, of which waited for: 4 -> 1; matrix products, arithmetic and copies ran while one was open for 6% -> 0% of each run, Pallas kernels for 0% -> 0%
where the time goes in v1:
time: 194 us; the launch traced here: 193 us
  blocking collectives  75.4 us (39%)
  waiting for transfers between devices  47.4 us (24%)
  Pallas kernels  33.9 us (17%)
  local copies, waits for them, and re-layouts  16.9 us (9%)
  other arithmetic  7.64 us (4%)
  matrix products  6.65 us (3%)
  starting transfers between devices  5.16 us (3%)
    all_to_all x1, blocking collectives, per_device(): lax.all_to_all(buffer.reshape(expert_count, capacity, width), ('sp', 'tp'...  75.4 us
    all_to_all x1, waiting for transfers between devices, per_device(): lax.all_to_all(result, ('sp', 'tp'), split_axis=0, concat_axis=0, tiled=T...  47.4 us
    pallas_call x1, Pallas kernels, attend(): pl.pallas_call(functools.partial(attend_kernel, n_sp, n_tp, chunks), out_...  33.9 us
    dot_general x1, matrix products, expert_rows(): jnp.dot(hidden, down_w, preferred_element_type=jnp.float32)  5.95 us
    all_to_all x1, starting transfers between devices, per_device(): lax.all_to_all(result, ('sp', 'tp'), split_axis=0, concat_axis=0, tiled=T...  5.16 us
    reduce_sum x1, other arithmetic, per_device(): moe = jnp.sum(route_weight[:, :, None] * picked.astype(jnp.float32), axis=1)  4.84 us
    scatter x1, local copies, waits for them, and re-layouts, per_device(): buffer = jnp.zeros((expert_count * capacity, width), jnp.bfloat16).at[slo...  4.35 us
    gather x1, local copies, waits for them, and re-layouts, per_device(): picked = returned.reshape(-1, width)[slots].reshape(local_rows, TOPK, width)  4.06 us
  transfers between devices with their start and end apart: 1, of which 1 were waited for; matrix products, arithmetic and copies ran while one was open for 0% of the time, Pallas kernels for 0%

profile of v1, /device:TPU:11, one launch (start us, length us, event | category | flops | bytes accessed | tf_op | source)
XLA Modules:
  0.0 193.1 jit_solution(10625298197683501767)
XLA Ops:
  0.0 0.0 copy-start
  0.0 0.9 copy.22
  0.9 0.7 broadcast_multiply_fusion
  1.6 33.9 %attend.1 = bf16[64,4096]{1,0:T(8,128)(2,1)} custom-call(f32[4]{0:T(128)} %off_ref.1, bf16[256,512]{1,0:T(8,128)(2,1)} %q_ref.1, bf16[256,512]{1,0:T(8,128)(2,1)} %k_ref.1, bf16[256,512]{1,0:T(8,128)(2,1)} %v_ref.1, f32[1,4096]{1,0:T(1,128)} %bitcast.33, f32[1,4096]{1,0:T(1,128)} %bitcast.34, bf16[64,4096]{1,0:T(8,128)(2,1)} %res_hbm.1, bf16[512,4096]{1,0:T(8,128)(2,1)} %w_hbm.1), custom_call_target="tpu_custom_call" | custom-call | tf_op jit(solution)/shard_map/attend/pallas_call | solution.py:237
  35.5 2.0 %broadcast_in_dim.11 = bf16[64,2,4096]{2,1,0:T(2,128)(2,1)S(1)} broadcast(bf16[64,4096]{1,0:T(8,128)(2,1)} %attend.1), dimensions={0,2} | broadcast | bytes 1572864 | tf_op jit(solution)/shard_map/broadcast_in_dim | solution.py:320
  37.5 1.2 reshape.110
  38.8 0.1 eq.15
  38.9 0.1 fusion.22
  39.0 0.2 reduce_window_sum.11
  39.2 0.2 select_reduce_fusion
  39.4 0.1 copy.21
  39.4 0.1 mul.78
  39.6 4.3 %scatter_custom_fusion = bf16[256,4096]{1,0:T(8,128)(2,1)} fusion(s32[128]{0:T(128)S(1)} %fusion.23, bf16[128,4096]{1,0:T(8,128)(2,1)} %reshape.110, bf16[]{:T(256)} %constant.6.clone.1), kind=kCustom, calls=%fused_computation.13 | custom fusion | bytes 2097664 | tf_op jit(solution)/shard_map/scatter | solution.py:320
  44.0 0.0 copy-start.3
  44.0 75.4 %all_to_all.10 = bf16[16,16,4096]{2,1,0:T(8,128)(2,1)S(1)} all-to-all(bf16[16,16,4096]{2,1,0:T(8,128)(2,1)} %bitcast.31), channel_id=1, replica_groups=mesh['grp'=2,'sp'=4,'tp'=4] {'sp','tp'}, dimensions={0} | all-to-all | bytes 4194304 | tf_op jit(solution)/shard_map/all_to_all | solution.py:322
  119.4 0.0 copy-start.1
  119.4 1.3 copy-done.1
  120.7 0.0 copy-done.3
  120.7 0.7 fusion.3
  121.4 0.0 copy-done
  121.4 5.9 %convolution_convert_fusion = bf16[256,4096]{1,0:T(8,128)(2,1)} fusion(bf16[1,256,4096]{2,1,0:T(8,128)(2,1)S(1)} %copy-done, bf16[256,4096]{1,0:T(8,128)(2,1)} %bitcast.30, bf16[1,4096,256]{2,1,0:T(8,128)(2,1)} %param.30, f32[256,256]{1,0:T(8,128)S(1)} %fusion.3), kind=kOutput, calls=%fused_computation.2 | convolution fusion | flops 1075183616 | bytes 8650752 | tf_op jit(solution)/shard_map/dot_general | solution.py:288
  127.3 0.0 copy-start.6
  127.3 0.0 copy-start.7
  127.3 5.2 %all-to-all-start.1 = ((bf16[16,16,4096]{2,1,0:T(8,128)(2,1)}), bf16[16,16,4096]{2,1,0:T(8,128)(2,1)}, u32[]{:S(2)}, u32[]{:S(2)}) async-start(bf16[16,16,4096]{2,1,0:T(8,128)(2,1)} %bitcast.32), calls=%async_computation.1 | async-start | bytes 4194304 | tf_op jit(solution)/shard_map/all_to_all | solution.py:332
  132.5 0.0 copy-done.6
  132.5 0.0 copy-done.7
  132.6 0.1 copy.20
  132.7 47.4 %all-to-all-done.1 = bf16[16,16,4096]{2,1,0:T(8,128)(2,1)} async-done(((bf16[16,16,4096]{2,1,0:T(8,128)(2,1)}), bf16[16,16,4096]{2,1,0:T(8,128)(2,1)}, u32[]{:S(2)}, u32[]{:S(2)}) %all-to-all-start.1) | async-done | bytes 2097184 | tf_op jit(solution)/shard_map/all_to_all | solution.py:332
  180.0 4.1 %gather_fusion = bf16[128,4096]{1,0:T(8,128)(2,1)S(1)} fusion(bf16[256,4096]{1,0:T(8,128)(2,1)} %bitcast.10, s32[1024]{0:T(1024)S(1)} %pad_clamp_fusion), kind=kCustom, calls=%fused_computation | custom fusion | bytes 2097664 | tf_op jit(solution)/shard_map/gather | solution.py:333
  184.1 2.4 %reshape.97 = f32[64,2,4096]{2,1,0:T(2,128)} reshape(bf16[128,4096]{1,0:T(8,128)(2,1)S(1)} %gather_fusion) | data formatting | bytes 3145728 | tf_op jit(solution)/shard_map/convert_element_type | solution.py:337
  186.5 0.0 copy-start.2
  186.5 4.8 %multiply_reduce_fusion = f32[64,4096]{1,0:T(8,128)S(1)} fusion(f32[64,2,4096]{2,1,0:T(2,128)} %reshape.97, f32[64,2]{1,0:T(8,128)S(1)} %copy.20), kind=kLoop, calls=%fused_computation.8 | loop fusion | flops 786432 | bytes 3146240 | tf_op jit(solution)/shard_map/reduce_sum | solution.py:337
  191.3 0.0 copy-done.2
  191.3 0.0 copy-start.4
  191.3 0.0 copy-start.5
  191.3 0.2 fusion.15
  191.6 0.3 multiply_reduce_fusion.1
  191.9 0.1 copy-done.4
  192.0 0.0 copy-done.5
  192.1 1.1 add_convert_fusion
  (6 shorter events, 0.0 us)
Async XLA Ops:
  0.0 121.4 %copy-start = (bf16[1,256,4096]{2,1,0:T(8,128)(2,1)S(1)}, bf16[1,256,4096]{2,1,0:T(8,128)(2,1)}, u32[]{:S(2)}) copy-start(bf16[1,256,4096]{2,1,0:T(8,128)(2,1)} %param.31) | copy-start | bytes 6291460
  44.0 76.7 %copy-start.3 = (bf16[1,4096,256]{2,1,0:T(8,128)(2,1)S(1)}, bf16[1,4096,256]{2,1,0:T(8,128)(2,1)}, u32[]{:S(2)}) copy-start(bf16[1,4096,256]{2,1,0:T(8,128)(2,1)} %param.29) | copy-start | bytes 6291460
  119.4 1.3 copy-start.1
  127.3 5.2 %copy-start.6 = (f32[64,2]{0,1:T(2,128)S(1)}, f32[64,2]{0,1:T(2,128)}, u32[]{:S(2)}) copy-start(f32[64,2]{0,1:T(2,128)} %param.27) | copy-start | bytes 1540
  127.3 5.2 %copy-start.7 = (f32[64]{0:T(128)S(1)}, f32[64]{0:T(128)}, u32[]{:S(2)}) copy-start(f32[64]{0:T(128)} %param.26) | copy-start | bytes 772
  127.3 52.7 %all-to-all-start.1 = ((bf16[16,16,4096]{2,1,0:T(8,128)(2,1)}), bf16[16,16,4096]{2,1,0:T(8,128)(2,1)}, u32[]{:S(2)}, u32[]{:S(2)}) async-start(bf16[16,16,4096]{2,1,0:T(8,128)(2,1)} %bitcast.32), calls=%async_computation.1 | async-start | bytes 4194304 | tf_op jit(solution)/shard_map/all_to_all | solution.py:332
  186.5 4.9 %copy-start.2 = (bf16[64,4096]{1,0:T(8,128)(2,1)S(1)}, bf16[64,4096]{1,0:T(8,128)(2,1)}, u32[]{:S(2)}) copy-start(bf16[64,4096]{1,0:T(8,128)(2,1)} %attend.1) | copy-start | bytes 1572868
  191.3 0.7 copy-start.4
  191.3 0.7 copy-start.5

commit v2 on v1

--- a/solution.py
+++ b/solution.py
@@ -266,26 +266,326 @@
     )(offsets, queries, keys, values, gain[None], shift[None], residual, out_weight)
 
 
-def layer_norm(rows, gain, shift):
-    mean = jnp.mean(rows, axis=-1, keepdims=True)
-    centred = rows - mean
-    variance = jnp.mean(centred * centred, axis=-1, keepdims=True)
-    return centred * lax.rsqrt(variance + norm_eps) * gain + shift
-
-
-def slot_index(routes, expert_count, capacity):
-    flat = routes.reshape(-1)
-    onehot = (flat[:, None] == jnp.arange(expert_count, dtype=jnp.int32)[None, :]).astype(jnp.int32)
-    earlier = jnp.cumsum(onehot, axis=0) - onehot
-    rank = jnp.sum(earlier * onehot, axis=1)
-    return flat * capacity + rank
-
-
-def expert_rows(rows, gate_w, up_w, down_w):
-    gate = jnp.dot(rows, gate_w, preferred_element_type=jnp.float32)
-    upper = jnp.dot(rows, up_w, preferred_element_type=jnp.float32)
-    hidden = (jax.nn.silu(gate) * upper).astype(jnp.bfloat16)
-    return jnp.dot(hidden, down_w, preferred_element_type=jnp.float32).astype(jnp.bfloat16)
+def experts_kernel(
+    n_sp,
+    n_tp,
+    slots,
+    extra,
+    x_ref,
+    routes_ref,
+    prob_ref,
+    logit_ref,
+    gain_ref,
+    shift_ref,
+    gate_hbm,
+    up_hbm,
+    down_hbm,
+    out_ref,
+    w_in,
+    w_out,
+    place,
+    outbox,
+    inbox,
+    partial,
+    near_in,
+    far_out,
+    far_in,
+    done,
+    returned,
+    rows_ref,
+    load_sem,
+    zs,
+    zr,
+    fs,
+    fr,
+    ns,
+    nr,
+    ps,
+    pr,
+    qs,
+    qr,
+    bs,
+    br,
+):
+    me = lax.axis_index("sp")
+    t = lax.axis_index("tp")
+    near = t + 1 - 2 * lax.rem(t, 2)
+    far = lax.rem(t + 2, 4)
+    across = lax.rem(near + 2, 4)
+    local, width = x_ref.shape
+    hidden_width = w_out.shape[0]
+    count = n_sp * n_tp
+    f32, bf16 = jnp.float32, jnp.bfloat16
+    step_cols = 1024 if width % 1024 == 0 else width
+
+    loads = [
+        pltpu.make_async_copy(gate_hbm.at[0], w_in.at[:, :hidden_width], load_sem.at[0]),
+        pltpu.make_async_copy(up_hbm.at[0], w_in.at[:, hidden_width:], load_sem.at[1]),
+        pltpu.make_async_copy(down_hbm.at[0], w_out, load_sem.at[2]),
+    ]
+    for load in loads:
+        load.start()
+
+    barrier = pltpu.get_barrier_semaphore()
+    for step in range(1, n_sp):
+        pl.semaphore_signal(
+            barrier, inc=1, device_id={"sp": lax.rem(me + step, n_sp)}, device_id_type=MESH
+        )
+    for partner in (near, far):
+        pl.semaphore_signal(barrier, inc=1, device_id={"tp": partner}, device_id_type=MESH)
+
+    first, second = routes_ref[:, 0:1], routes_ref[:, 1:2]
+    line = lax.broadcasted_iota(jnp.int32, (local, n_sp), 1)
+    member = jnp.where(
+        (line == first // n_tp) | (line == second // n_tp), 1.0, 0.0
+    ).astype(bf16)
+    before = jnp.where(
+        lax.broadcasted_iota(jnp.int32, (local, local), 1)
+        < lax.broadcasted_iota(jnp.int32, (local, local), 0),
+        1.0,
+        0.0,
+    ).astype(bf16)
+    rank = jnp.dot(before, member, preferred_element_type=f32).astype(bf16)
+    total = n_sp * slots
+    spread = jnp.where(
+        lax.broadcasted_iota(jnp.int32, (n_sp, total), 1) // slots
+        == lax.broadcasted_iota(jnp.int32, (n_sp, total), 0),
+        1.0,
+        0.0,
+    ).astype(bf16)
+    member_wide = jnp.dot(member, spread, preferred_element_type=f32)
+    rank_wide = jnp.dot(rank, spread, preferred_element_type=f32)
+    slot_id = lax.rem(lax.broadcasted_iota(jnp.int32, (local, total), 1), slots).astype(f32)
+    place[...] = jnp.where((member_wide > 0.5) & (rank_wide == slot_id), 1.0, 0.0).astype(bf16)
+
+    difference = logit_ref[:, 0:1] - logit_ref[:, 1:2]
+    weight_one = prob_ref[...] / (1.0 + jnp.exp(-difference))
+    weight_two = prob_ref[...] / (1.0 + jnp.exp(difference))
+    lane = lax.broadcasted_iota(jnp.int32, (local, extra), 1)
+    name = lax.rem(lane, count)
+    value = jnp.where(name == first, weight_one, 0.0) + jnp.where(name == second, weight_two, 0.0)
+    value = jnp.where(lane < 2 * count, value, 0.0)
+    high = value.astype(bf16)
+    low = (value - high.astype(f32)).astype(bf16)
+    tags = jnp.where(lane < count, high.astype(f32), low.astype(f32)).astype(bf16)
+
+    def placed(rows):
+        return lax.dot_general(
+            place[...], rows, (((0,), (0,)), ((), ())), preferred_element_type=f32
+        ).astype(bf16)
+
+    for c in range(0, width, step_cols):
+        outbox[:, :, c : c + step_cols] = placed(x_ref[:, c : c + step_cols]).reshape(
+            n_sp, slots, step_cols
+        )
+    outbox[:, :, width:] = placed(tags).reshape(n_sp, slots, extra)
+
+    pl.semaphore_wait(barrier, n_sp + 1)
+
+    def go(z):
+        return remote(outbox.at[z], inbox.at[me, t], zs.at[z], zr.at[me], {"sp": z})
+
+    def come(z):
+        return remote(outbox.at[z], inbox.at[z, t], zs.at[z], zr.at[z], {"sp": z})
+
+    def to_far(z):
+        return remote(inbox.at[z, t], inbox.at[z, t], fs.at[z], fr.at[z], {"tp": far})
+
+    def to_near(z, i):
+        block = inbox.at[z, (t, far)[i]]
+        return remote(block, block, ns.at[z, i], nr.at[z, i], {"tp": near})
+
+    def part_near(z, i):
+        return remote(
+            partial.at[z, (near, across)[i]],
+            near_in.at[z, i],
+            ps.at[z, i],
+            pr.at[z, i],
+            {"tp": near},
+        )
+
+    def part_far(z):
+        return remote(far_out.at[z], far_in.at[z], qs.at[z], qr.at[z], {"tp": far})
+
+    def back(z):
+        return remote(done.at[z], returned.at[me], bs.at[z], br.at[me], {"sp": z})
+
+    def back_in(z):
+        return remote(done.at[z], returned.at[z], bs.at[z], br.at[z], {"sp": z})
+
+    def send_out(step, _):
+        go(lax.rem(me + step, n_sp)).start()
+        return 0
+
+    lax.fori_loop(1, n_sp, send_out, 0)
+    inbox[me, t] = outbox[me]
+
+    def run_experts(z):
+        rows = inbox[z].reshape(n_tp * slots, width + extra)
+        own = me * n_tp + t
+        tag = rows[:, width:].astype(f32)
+        tag_lane = lax.broadcasted_iota(jnp.int32, tag.shape, 1)
+        weight = jnp.sum(
+            jnp.where((tag_lane == own) | (tag_lane == own + count), tag, 0.0),
+            axis=1,
+            keepdims=True,
+        )
+        both = jnp.dot(rows[:, :width], w_in[...], preferred_element_type=f32)
+        gate, upper = both[:, :hidden_width], both[:, hidden_width:]
+        hidden = (gate / (1.0 + jnp.exp(-gate)) * upper).astype(bf16)
+        for c in range(0, width, step_cols):
+            part = jnp.dot(
+                hidden, w_out[:, c : c + step_cols], preferred_element_type=f32
+            ).astype(bf16)
+            partial[z, :, :, c : c + step_cols] = (
+                (part.astype(f32) * weight).astype(bf16).reshape(n_tp, slots, step_cols)
+            )
+
+    def turn(step, _):
+        @pl.when(step < n_sp)
+        def _():
+            z = lax.rem(me - step + n_sp, n_sp)
+
+            @pl.when(step > 0)
+            def _():
+                come(z).wait_recv()
+
+            to_far(z).start()
+            to_near(z, 0).start()
+
+        @pl.when(step == 1)
+        def _():
+            for load in loads:
+                load.wait()
+
+        @pl.when((step >= 1) & (step <= n_sp))
+        def _():
+            z = lax.rem(me - step + 1 + n_sp, n_sp)
+            to_far(z).wait_recv()
+            to_near(z, 1).start()
+            to_near(z, 0).wait_recv()
+            to_near(z, 1).wait_recv()
+            run_experts(z)
+            part_near(z, 1).start()
+            part_near(z, 0).start()
+            part_near(z, 1).wait_recv()
+            far_out[z] = (partial[z, far].astype(f32) + near_in[z, 1].astype(f32)).astype(bf16)
+            part_far(z).start()
+            part_near(z, 0).wait_recv()
+
+        @pl.when(step >= 2)
+        def _():
+            z = lax.rem(me - step + 2 + n_sp, n_sp)
+            part_far(z).wait_recv()
+            whole = (
+                partial[z, t].astype(f32) + near_in[z, 0].astype(f32) + far_in[z].astype(f32)
+            ).astype(bf16)
+
+            @pl.when(z == me)
+            def _():
+                returned[me] = whole
+
+            @pl.when(z != me)
+            def _():
+                done[z] = whole
+                back(z).start()
+
+        return 0
+
+    lax.fori_loop(0, n_sp + 2, turn, 0)
+
+    def collect(step, _):
+        back_in(lax.rem(me + step, n_sp)).wait_recv()
+        return 0
+
+    lax.fori_loop(1, n_sp, collect, 0)
+    for c in range(0, width, step_cols):
+        span = slice(c, c + step_cols)
+        moe = jnp.dot(
+            place[...], returned[:, :, span].reshape(total, step_cols), preferred_element_type=f32
+        )
+        rows_ref[:, span] = residual_scale * x_ref[:, span].astype(f32) + moe
+    out_ref[...] = norm_rows(rows_ref[...], gain_ref[...], shift_ref[...]).astype(bf16)
+
+    def drain(step, _):
+        z = lax.rem(me + step, n_sp)
+
+        @pl.when(step > 0)
+        def _():
+            go(z).wait_send()
+            back(z).wait_send()
+
+        to_far(z).wait_send()
+        part_far(z).wait_send()
+        for i in range(2):
+            to_near(z, i).wait_send()
+            part_near(z, i).wait_send()
+        return 0
+
+    lax.fori_loop(0, n_sp, drain, 0)
+
+
+def experts(normed, routes, group_prob, pair_logits, gain, shift, w_gate, w_up, w_down):
+    n_sp, n_tp = lax.axis_size("sp"), lax.axis_size("tp")
+    assert n_tp == 4
+    local, width = normed.shape
+    hidden = w_down.shape[1]
+    count = n_sp * n_tp
+    group = count // GROUPS
+    capacity = local // group
+    slots = n_tp * capacity
+    if n_tp % group == 0:
+        slots = slots // TOPK
+    extra = -(-2 * count // 128) * 128
+    vmem = pl.BlockSpec(memory_space=pltpu.VMEM)
+    hbm = pl.BlockSpec(memory_space=pl.ANY)
+    dma = pltpu.SemaphoreType.DMA
+    bf16, f32 = jnp.bfloat16, jnp.float32
+    return pl.pallas_call(
+        functools.partial(experts_kernel, n_sp, n_tp, slots, extra),
+        out_shape=jax.ShapeDtypeStruct((local, width), bf16),
+        in_specs=[vmem] * 6 + [hbm] * 3,
+        out_specs=vmem,
+        scratch_shapes=[
+            pltpu.VMEM((width, 2 * hidden), bf16),
+            pltpu.VMEM((hidden, width), bf16),
+            pltpu.VMEM((local, n_sp * slots), bf16),
+            pltpu.VMEM((n_sp, slots, width + extra), bf16),
+            pltpu.VMEM((n_sp, n_tp, slots, width + extra), bf16),
+            pltpu.VMEM((n_sp, n_tp, slots, width), bf16),
+            pltpu.VMEM((n_sp, 2, slots, width), bf16),
+            pltpu.VMEM((n_sp, slots, width), bf16),
+            pltpu.VMEM((n_sp, slots, width), bf16),
+            pltpu.VMEM((n_sp, slots, width), bf16),
+            pltpu.VMEM((n_sp, slots, width), bf16),
+            pltpu.VMEM((local, width), f32),
+            dma((3,)),
+            dma((n_sp,)),
+            dma((n_sp,)),
+            dma((n_sp,)),
+            dma((n_sp,)),
+            dma((n_sp, 2)),
+            dma((n_sp, 2)),
+            dma((n_sp, 2)),
+            dma((n_sp, 2)),
+            dma((n_sp,)),
+            dma((n_sp,)),
+            dma((n_sp,)),
+            dma((n_sp,)),
+        ],
+        compiler_params=pltpu.CompilerParams(collective_id=1, has_side_effects=True),
+        name="experts",
+    )(
+        normed,
+        routes,
+        group_prob[:, None],
+        pair_logits,
+        gain[None],
+        shift[None],
+        w_gate,
+        w_up,
+        w_down,
+    )
 
 
 def per_device(
@@ -309,35 +609,9 @@
     normed = attend(
         queries, keys, values, offsets, residual, out_weight, gain_one, shift_one
     )
-    local_rows = residual.shape[0]
-    width = normed.shape[1]
-    expert_count = lax.axis_size("sp") * lax.axis_size("tp")
-    capacity = local_rows // (expert_count // GROUPS)
-    slots = slot_index(routes, expert_count, capacity)
-    buffer = (
-        jnp.zeros((expert_count * capacity, width), jnp.bfloat16)
-        .at[slots]
-        .set(jnp.repeat(normed, TOPK, axis=0))
+    return experts(
+        normed, routes, group_prob, pair_logits, gain_two, shift_two, w_gate, w_up, w_down
     )
-    arrived = lax.all_to_all(
-        buffer.reshape(expert_count, capacity, width),
-        ("sp", "tp"),
-        split_axis=0,
-        concat_axis=0,
-        tiled=True,
-    )
-    result = expert_rows(arrived.reshape(-1, width), w_gate[0], w_up[0], w_down[0]).reshape(
-        expert_count, capacity, width
-    )
-    returned = lax.all_to_all(result, ("sp", "tp"), split_axis=0, concat_axis=0, tiled=True)
-    picked = returned.reshape(-1, width)[slots].reshape(local_rows, TOPK, width)
-    difference = pair_logits[:, 0] - pair_logits[:, 1]
-    pair_weight = jnp.stack([jax.nn.sigmoid(difference), jax.nn.sigmoid(-difference)], axis=1)
-    route_weight = group_prob[:, None] * pair_weight
-    moe = jnp.sum(route_weight[:, :, None] * picked.astype(jnp.float32), axis=1)
-    return layer_norm(
-        residual_scale * normed.astype(jnp.float32) + moe, gain_two, shift_two
-    ).astype(jnp.bfloat16)
 
 
 def solution(mesh):

time: 194 us -> 137 us (0.71)
  the two profiles are of different devices: /device:TPU:11 before, /device:TPU:0 now
where the time goes in v2:
time: 137 us; the launch traced here: 136 us
  Pallas kernels  130 us (95%)
  local copies, waits for them, and re-layouts  5.97 us (4%)
    pallas_call x1, Pallas kernels, experts(): pl.pallas_call(functools.partial(experts_kernel, n_sp, n_tp, slots, extra...  105 us
    pallas_call x1, Pallas kernels, attend(): pl.pallas_call(functools.partial(attend_kernel, n_sp, n_tp, chunks), out_...  25.3 us
    unnamed x3, local copies, waits for them, and re-layouts  4.62 us

profile of v2, /device:TPU:0, one launch (start us, length us, event | category | flops | bytes accessed | tf_op | source)
XLA Modules:
  0.0 136.3 jit_solution(17864580579218709828)
XLA Ops:
  0.0 1.3 copy.18.prob_ref
  1.3 1.4 %copy.19.logit_ref = f32[64,2]{1,0:T(8,128)} copy(f32[64,2]{0,1:T(2,128)} %param.27) | data formatting | bytes 1024 | tf_op args[11]
  2.7 1.4 %copy.17.routes_ref = s32[64,2]{1,0:T(8,128)} copy(s32[64,2]{0,1:T(2,128)} %param.28) | data formatting | bytes 1024 | tf_op args[12]
  4.1 25.3 %attend.1.x_ref = bf16[64,4096]{1,0:T(8,128)(2,1)} custom-call(f32[4]{0:T(128)} %off_ref.1, bf16[256,512]{1,0:T(8,128)(2,1)} %q_ref.1, bf16[256,512]{1,0:T(8,128)(2,1)} %k_ref.1, bf16[256,512]{1,0:T(8,128)(2,1)} %v_ref.1, f32[1,4096]{1,0:T(1,128)} %bitcast.5, f32[1,4096]{1,0:T(1,128)} %bitcast.6, bf16[64,4096]{1,0:T(8,128)(2,1)} %res_hbm.1, ...), custom_call_target="tpu_custom_call" | custom-call | tf_op jit(solution)/shard_map/attend/pallas_call | solution.py:237
  29.4 105.0 %experts.1 = bf16[64,4096]{1,0:T(8,128)(2,1)} custom-call(bf16[64,4096]{1,0:T(8,128)(2,1)} %attend.1.x_ref, s32[64,2]{1,0:T(8,128)} %copy.17.routes_ref, f32[64,1]{1,0:T(8,128)} %copy.18.prob_ref, f32[64,2]{1,0:T(8,128)} %copy.19.logit_ref, f32[1,4096]{1,0:T(1,128)} %bitcast.7, f32[1,4096]{1,0:T(1,128)} %bitcast.8, bf16[1,4096,256]{2,1,0:T(8,128)(2,1)} %gate_hbm.1, ...), custom_call_target="tpu_custom_call" | custom-call | tf_op jit(solution)/shard_map/experts/pallas_call | solution.py:544
  134.4 1.9 %copy.21 = bf16[64,4096]{1,0:T(8,128)(2,1)} copy(bf16[64,4096]{1,0:T(8,128)(2,1)} %experts.1) | data formatting | bytes 1048576

commit v3 on v2

--- a/solution.py
+++ b/solution.py
@@ -334,7 +334,15 @@
     for partner in (near, far):
         pl.semaphore_signal(barrier, inc=1, device_id={"tp": partner}, device_id_type=MESH)
 
-    first, second = routes_ref[:, 0:1], routes_ref[:, 1:2]
+    same = lax.broadcasted_iota(jnp.int32, (local, local), 0) == lax.broadcasted_iota(
+        jnp.int32, (local, local), 1
+    )
+
+    def column(line_of):
+        return jnp.sum(jnp.where(same, line_of, jnp.zeros_like(line_of)), axis=1, keepdims=True)
+
+    first, second = column(routes_ref[0:1, :]), column(routes_ref[1:2, :])
+    prob = column(prob_ref[...])
     line = lax.broadcasted_iota(jnp.int32, (local, n_sp), 1)
     member = jnp.where(
         (line == first // n_tp) | (line == second // n_tp), 1.0, 0.0
@@ -358,9 +366,9 @@
     slot_id = lax.rem(lax.broadcasted_iota(jnp.int32, (local, total), 1), slots).astype(f32)
     place[...] = jnp.where((member_wide > 0.5) & (rank_wide == slot_id), 1.0, 0.0).astype(bf16)
 
-    difference = logit_ref[:, 0:1] - logit_ref[:, 1:2]
-    weight_one = prob_ref[...] / (1.0 + jnp.exp(-difference))
-    weight_two = prob_ref[...] / (1.0 + jnp.exp(difference))
+    difference = column(logit_ref[0:1, :] - logit_ref[1:2, :])
+    weight_one = prob / (1.0 + jnp.exp(-difference))
+    weight_two = prob / (1.0 + jnp.exp(difference))
     lane = lax.broadcasted_iota(jnp.int32, (local, extra), 1)
     name = lax.rem(lane, count)
     value = jnp.where(name == first, weight_one, 0.0) + jnp.where(name == second, weight_two, 0.0)
@@ -413,11 +421,19 @@
     def back_in(z):
         return remote(done.at[z], returned.at[z], bs.at[z], br.at[z], {"sp": z})
 
+    def pair(step):
+        other, scale = 0, 1
+        while scale < n_sp:
+            bit = lax.rem(me // scale + step // scale, 2)
+            other = other + bit * scale
+            scale = 2 * scale
+        return other
+
     def send_out(step, _):
-        go(lax.rem(me + step, n_sp)).start()
+        go(pair(step)).start()
         return 0
 
-    lax.fori_loop(1, n_sp, send_out, 0)
+    lax.fori_loop(1, min(3, n_sp), send_out, 0)
     inbox[me, t] = outbox[me]
 
     def run_experts(z):
@@ -444,11 +460,15 @@
     def turn(step, _):
         @pl.when(step < n_sp)
         def _():
-            z = lax.rem(me - step + n_sp, n_sp)
+            z = pair(step)
 
             @pl.when(step > 0)
             def _():
                 come(z).wait_recv()
+
+            @pl.when((step > 1) & (step < n_sp - 1))
+            def _():
+                go(pair(step + 1)).start()
 
             to_far(z).start()
             to_near(z, 0).start()
@@ -460,7 +480,7 @@
 
         @pl.when((step >= 1) & (step <= n_sp))
         def _():
-            z = lax.rem(me - step + 1 + n_sp, n_sp)
+            z = pair(step - 1)
             to_far(z).wait_recv()
             to_near(z, 1).start()
             to_near(z, 0).wait_recv()
@@ -475,7 +495,7 @@
 
         @pl.when(step >= 2)
         def _():
-            z = lax.rem(me - step + 2 + n_sp, n_sp)
+            z = pair(step - 2)
             part_far(z).wait_recv()
             whole = (
                 partial[z, t].astype(f32) + near_in[z, 0].astype(f32) + far_in[z].astype(f32)
@@ -495,7 +515,7 @@
     lax.fori_loop(0, n_sp + 2, turn, 0)
 
     def collect(step, _):
-        back_in(lax.rem(me + step, n_sp)).wait_recv()
+        back_in(pair(step)).wait_recv()
         return 0
 
     lax.fori_loop(1, n_sp, collect, 0)
@@ -508,7 +528,7 @@
     out_ref[...] = norm_rows(rows_ref[...], gain_ref[...], shift_ref[...]).astype(bf16)
 
     def drain(step, _):
-        z = lax.rem(me + step, n_sp)
+        z = pair(step)
 
         @pl.when(step > 0)
         def _():
@@ -527,7 +547,7 @@
 
 def experts(normed, routes, group_prob, pair_logits, gain, shift, w_gate, w_up, w_down):
     n_sp, n_tp = lax.axis_size("sp"), lax.axis_size("tp")
-    assert n_tp == 4
+    assert n_tp == 4 and n_sp & (n_sp - 1) == 0
     local, width = normed.shape
     hidden = w_down.shape[1]
     count = n_sp * n_tp
@@ -577,9 +597,9 @@
         name="experts",
     )(
         normed,
-        routes,
-        group_prob[:, None],
-        pair_logits,
+        routes.T,
+        group_prob[None],
+        pair_logits.T,
         gain[None],
         shift[None],
         w_gate,

time: 137 us -> 130 us (0.949)
  the two profiles are of different devices: /device:TPU:0 before, /device:TPU:11 now
where the time goes in v3:
time: 130 us; the launch traced here: 129 us
  Pallas kernels  127 us (98%)
  local copies, waits for them, and re-layouts  1.87 us (1%)
    pallas_call x1, Pallas kernels, experts(): pl.pallas_call(functools.partial(experts_kernel, n_sp, n_tp, slots, extra...  93.1 us
    pallas_call x1, Pallas kernels, attend(): pl.pallas_call(functools.partial(attend_kernel, n_sp, n_tp, chunks), out_...  33.9 us

profile of v3, /device:TPU:11, one launch (start us, length us, event | category | flops | bytes accessed | tf_op | source)
XLA Modules:
  0.0 128.9 jit_solution(12403605173533778758)
XLA Ops:
  0.0 33.9 %attend.1.x_ref = bf16[64,4096]{1,0:T(8,128)(2,1)} custom-call(f32[4]{0:T(128)} %off_ref.1, bf16[256,512]{1,0:T(8,128)(2,1)} %q_ref.1, bf16[256,512]{1,0:T(8,128)(2,1)} %k_ref.1, bf16[256,512]{1,0:T(8,128)(2,1)} %v_ref.1, f32[1,4096]{1,0:T(1,128)} %bitcast.7, f32[1,4096]{1,0:T(1,128)} %bitcast.8, bf16[64,4096]{1,0:T(8,128)(2,1)} %res_hbm.1, ...), custom_call_target="tpu_custom_call" | custom-call | tf_op jit(solution)/shard_map/attend/pallas_call | solution.py:237
  33.9 93.1 %experts.1 = bf16[64,4096]{1,0:T(8,128)(2,1)} custom-call(bf16[64,4096]{1,0:T(8,128)(2,1)} %attend.1.x_ref, s32[2,64]{1,0:T(2,128)} %bitcast.11, f32[1,64]{1,0:T(1,128)} %bitcast.13, f32[2,64]{1,0:T(2,128)} %bitcast.12, f32[1,4096]{1,0:T(1,128)} %bitcast.9, f32[1,4096]{1,0:T(1,128)} %bitcast.10, bf16[1,4096,256]{2,1,0:T(8,128)(2,1)} %gate_hbm.1, ...), custom_call_target="tpu_custom_call" | custom-call | tf_op jit(solution)/shard_map/experts/pallas_call | solution.py:564
  127.0 1.9 %copy.18 = bf16[64,4096]{1,0:T(8,128)(2,1)} copy(bf16[64,4096]{1,0:T(8,128)(2,1)} %experts.1) | data formatting | bytes 1048576

commit v4 on v3

--- a/solution.py
+++ b/solution.py
@@ -466,9 +466,9 @@
             def _():
                 come(z).wait_recv()
 
-            @pl.when((step > 1) & (step < n_sp - 1))
+            @pl.when((step > 0) & (step < n_sp - 2))
             def _():
-                go(pair(step + 1)).start()
+                go(pair(step + 2)).start()
 
             to_far(z).start()
             to_near(z, 0).start()

time: 130 us -> 130 us (level)
  no operation moved by 1% of the time
where the time goes in v4:
time: 130 us; the launch traced here: 129 us
  Pallas kernels  127 us (98%)
  local copies, waits for them, and re-layouts  1.87 us (1%)
    pallas_call x1, Pallas kernels, experts(): pl.pallas_call(functools.partial(experts_kernel, n_sp, n_tp, slots, extra...  93.1 us
    pallas_call x1, Pallas kernels, attend(): pl.pallas_call(functools.partial(attend_kernel, n_sp, n_tp, chunks), out_...  33.9 us

profile of v4, /device:TPU:11, one launch (start us, length us, event | category | flops | bytes accessed | tf_op | source)
XLA Modules:
  0.0 128.9 jit_solution(1863401195858322958)
XLA Ops:
  0.0 33.9 %attend.1.x_ref = bf16[64,4096]{1,0:T(8,128)(2,1)} custom-call(f32[4]{0:T(128)} %off_ref.1, bf16[256,512]{1,0:T(8,128)(2,1)} %q_ref.1, bf16[256,512]{1,0:T(8,128)(2,1)} %k_ref.1, bf16[256,512]{1,0:T(8,128)(2,1)} %v_ref.1, f32[1,4096]{1,0:T(1,128)} %bitcast.7, f32[1,4096]{1,0:T(1,128)} %bitcast.8, bf16[64,4096]{1,0:T(8,128)(2,1)} %res_hbm.1, ...), custom_call_target="tpu_custom_call" | custom-call | tf_op jit(solution)/shard_map/attend/pallas_call | solution.py:237
  33.9 93.1 %experts.1 = bf16[64,4096]{1,0:T(8,128)(2,1)} custom-call(bf16[64,4096]{1,0:T(8,128)(2,1)} %attend.1.x_ref, s32[2,64]{1,0:T(2,128)} %bitcast.11, f32[1,64]{1,0:T(1,128)} %bitcast.13, f32[2,64]{1,0:T(2,128)} %bitcast.12, f32[1,4096]{1,0:T(1,128)} %bitcast.9, f32[1,4096]{1,0:T(1,128)} %bitcast.10, bf16[1,4096,256]{2,1,0:T(8,128)(2,1)} %gate_hbm.1, ...), custom_call_target="tpu_custom_call" | custom-call | tf_op jit(solution)/shard_map/experts/pallas_call | solution.py:564
  127.0 1.9 %copy.18 = bf16[64,4096]{1,0:T(8,128)(2,1)} copy(bf16[64,4096]{1,0:T(8,128)(2,1)} %experts.1) | data formatting | bytes 1048576
